TPU v7x, 32 devices: a whole 2x2x4 slice. The times are simulated.
32 devices in a mesh: ep: 8 (over z, x), tp: 4 (over y, core).
Axes of the slice: x: 2, y: 2, z: 4, core: 2. Of those that a mesh axis runs over, the one named last changes fastest.
Arguments:
- x_attend: bfloat16 [4096, 2048], P('ep'), may hold values from -6 to 6
- attend_gain: float32 [2048], replicated, may hold values from 0.1 to 1.9
- w_query: bfloat16 [2048, 1024], P(None, 'tp'), may hold values from -0.125 to 0.125
- w_key: bfloat16 [2048, 512], P(None, 'tp'), may hold values from -0.125 to 0.125
- w_value: bfloat16 [2048, 512], P(None, 'tp'), may hold values from -0.125 to 0.125
- query_gain: float32 [64], replicated, may hold values from 0.1 to 1.9
- key_gain: float32 [64], replicated, may hold values from 0.1 to 1.9
- sink_logit: float32 [16], P('tp'), may hold values from 4 to 8
- w_output: bfloat16 [1024, 2048], P('tp'), may hold values from -1.5 to 1.5
- x_experts: bfloat16 [3072, 2048], P('ep'), may hold values from -6 to 6
- expert_gain: float32 [2048], replicated, may hold values from 0.1 to 1.9
- routes: int32 [3072, 2], P('ep'), may hold values from 0 to 7, all different within a row; in each aligned block of 384 rows (0 to 383, 384 to 767, ...) at most 144 rows name the same one
- group_prob: float32 [3072], P('ep'), may hold values from 0.3 to 1
- expert_prob: float32 [3072, 2], P('ep'), may hold values from 0.05 to 1
- w_gate: bfloat16 [8, 2048, 1024], P('ep', None, 'tp'), may hold values from -0.125 to 0.125
- w_up: bfloat16 [8, 2048, 1024], P('ep', None, 'tp'), may hold values from -0.125 to 0.125
- w_down: bfloat16 [8, 1024, 2048], P('ep', 'tp'), may hold values from -0.1875 to 0.1875
Outputs:
- attend_out: bfloat16 [4096, 2048], P(('ep', 'tp'))
- expert_out: bfloat16 [3072, 2048], P('ep', 'tp')
Inputs may be any that keep to these rules, and one draw needn't show every extreme that they name: `routes`: each row names 2 different experts. Among the rows of one device no expert is named more than 144 times, and in every draw some expert is named exactly 144 times by one device's rows.
All inputs are finite; a program needn't handle non-finite values.
Results may differ from a plain program's by a relative error of at most 0.012.
Values may be sent and summed in bfloat16 or wider, within the bound.
A program may use at most 64 MiB of HBM per device.

v0:
```python
import jax
import jax.numpy as jnp
from jax import lax
from jax.sharding import PartitionSpec as P

HEAD_DIM = 64
WINDOW = 128
GRID_W = 64
epsilon = 1e-06
rope_base = 10000.0


def extended(x, sides, width):
    for axis, dim in sides:
        peers, length = (lax.axis_size(axis), x.shape[dim])
        up = [(i, (i + 1) % peers) for i in range(peers - 1)]
        down = [(j, i) for i, j in up]
        last = lax.slice_in_dim(x, length - width, length, axis=dim)
        initial = lax.slice_in_dim(x, 0, width, axis=dim)
        before = lax.ppermute(last, axis, up)
        after = lax.ppermute(initial, axis, down)
        x = jnp.concatenate([before, x, after], axis=dim)
    return x


def rms_scale(inputs, gain):
    values_f = inputs.astype(jnp.float32)
    scaled = values_f * lax.rsqrt(jnp.mean(values_f * values_f, axis=-1, keepdims=True) + epsilon)
    return (scaled * gain).astype(jnp.bfloat16)


def rope_tables(positions):
    grid_rows = (positions // GRID_W).astype(jnp.float32)
    grid_cols = (positions % GRID_W).astype(jnp.float32)
    half_dim = HEAD_DIM // 2
    inverse = rope_base ** (-jnp.arange(0, half_dim, 2, dtype=jnp.float32) / half_dim)
    angles = jnp.concatenate([grid_rows[:, None] * inverse, grid_cols[:, None] * inverse], axis=-1)
    return (jnp.cos(angles), jnp.sin(angles))


def head_norm_rope(projected, gain, cosine, sine_tab):
    scaled = (
        projected
        * lax.rsqrt(jnp.mean(projected * projected, axis=-1, keepdims=True) + epsilon)
        * gain
    )
    first_half, second_half = jnp.split(scaled, 2, axis=-1)
    cos_b = cosine[:, None, :]
    sin_b = sine_tab[:, None, :]
    turned = jnp.concatenate(
        [first_half * cos_b - second_half * sin_b, second_half * cos_b + first_half * sin_b],
        axis=-1,
    )
    return turned.astype(jnp.bfloat16)


def per_device(
    x_attend,
    attend_gain,
    w_query,
    w_key,
    w_value,
    query_gain,
    key_gain,
    sink_logit,
    w_output,
    x_experts,
    expert_gain,
    routes,
    group_prob,
    expert_prob,
    w_gate,
    w_up,
    w_down,
):
    tok_rows = x_attend.shape[0]
    model_width = x_attend.shape[1]
    heads_local = sink_logit.shape[0]
    kv_local = w_key.shape[1] // HEAD_DIM
    group = heads_local // kv_local
    offset = lax.axis_index("ep") * tok_rows
    positions = offset + jnp.arange(tok_rows, dtype=jnp.int32)
    cosine, sine_tab = rope_tables(positions)
    normed = rms_scale(x_attend, attend_gain)
    queries = head_norm_rope(
        jnp.dot(normed, w_query, preferred_element_type=jnp.float32).reshape(
            tok_rows, heads_local, HEAD_DIM
        ),
        query_gain,
        cosine,
        sine_tab,
    )
    key_rows = head_norm_rope(
        jnp.dot(normed, w_key, preferred_element_type=jnp.float32).reshape(
            tok_rows, kv_local, HEAD_DIM
        ),
        key_gain,
        cosine,
        sine_tab,
    )
    values = jnp.dot(normed, w_value, preferred_element_type=jnp.float32).astype(jnp.bfloat16)
    stacked = jnp.stack([key_rows.reshape(tok_rows, kv_local * HEAD_DIM), values], axis=0)
    padded = extended(stacked, (("ep", 1),), WINDOW)
    span_keys = padded[0].reshape(tok_rows + 2 * WINDOW, kv_local, HEAD_DIM)
    span_values = padded[1].reshape(tok_rows + 2 * WINDOW, kv_local, HEAD_DIM)
    scores = jnp.einsum(
        "qhgd,khd->hgqk",
        queries.reshape(tok_rows, kv_local, group, HEAD_DIM),
        span_keys,
        preferred_element_type=jnp.float32,
    ) * HEAD_DIM ** (-0.5)
    key_pos = offset - WINDOW + jnp.arange(tok_rows + 2 * WINDOW, dtype=jnp.int32)
    total_len = tok_rows * lax.axis_size("ep")
    in_window = (
        (jnp.abs(positions[:, None] - key_pos[None, :]) <= WINDOW)
        & (key_pos[None, :] >= 0)
        & (key_pos[None, :] < total_len)
    )
    scores = jnp.where(in_window[None, None], scores, -1e30)
    sink_col = sink_logit.reshape(kv_local, group)[:, :, None]
    peak = jnp.maximum(jnp.max(scores, axis=-1), sink_col)[..., None]
    weights = jnp.exp(scores - peak)
    denominator = jnp.sum(weights, axis=-1, keepdims=True) + jnp.exp(sink_col[..., None] - peak)
    probs = (weights / denominator).astype(jnp.bfloat16)
    attended = jnp.einsum("hgqk,khd->qhgd", probs, span_values, preferred_element_type=jnp.float32)
    attended = attended.astype(jnp.bfloat16).reshape(tok_rows, heads_local * HEAD_DIM)
    rows_in = attended
    attend_out = lax.psum_scatter(
        jnp.dot(rows_in, w_output, preferred_element_type=jnp.float32).astype(jnp.bfloat16),
        "tp",
        scatter_dimension=0,
        tiled=True,
    )
    moe_rows = x_experts.shape[0]
    top_count = routes.shape[1]
    experts_n = lax.axis_size("ep")
    tp_count = lax.axis_size("tp")
    capacity = max(2, (3 * moe_rows * top_count + 2 * experts_n - 1) // (2 * experts_n))
    moe_normed = rms_scale(x_experts, expert_gain)
    flat_ids = routes.reshape(-1)
    onehot = (flat_ids[:, None] == jnp.arange(experts_n, dtype=jnp.int32)[None, :]).astype(
        jnp.int32
    )
    rank_in = jnp.cumsum(onehot, axis=0) - onehot
    slot_pos = jnp.sum(rank_in * onehot, axis=1)
    dest_slot = flat_ids * capacity + slot_pos
    owner_tok = jnp.arange(moe_rows * top_count, dtype=jnp.int32) // top_count
    slot_tok = jnp.full((experts_n * capacity,), moe_rows, jnp.int32).at[dest_slot].set(owner_tok)
    gate_mat = w_gate[0]
    up_mat = w_up[0]
    down_mat = w_down[0]
    col_width = model_width // tp_count
    own_cols = lax.dynamic_slice_in_dim(moe_normed, lax.axis_index("tp") * col_width, col_width, 1)
    padded_rows = jnp.concatenate([own_cols, jnp.zeros((1, col_width), jnp.bfloat16)], axis=0)
    outgoing = padded_rows[slot_tok].reshape(experts_n, capacity, col_width)
    arrived = lax.all_to_all(outgoing, "ep", split_axis=0, concat_axis=0, tiled=True)
    col_piece = lax.all_gather(arrived, "tp", axis=2, tiled=True)
    rows_in = col_piece.reshape(experts_n * capacity, col_piece.shape[2])
    gate_act = jnp.dot(rows_in, gate_mat, preferred_element_type=jnp.float32)
    up_act = jnp.dot(rows_in, up_mat, preferred_element_type=jnp.float32)
    hidden = (jax.nn.silu(gate_act) * up_act).astype(jnp.bfloat16)
    partial_value = jnp.dot(hidden, down_mat, preferred_element_type=jnp.float32).astype(
        jnp.bfloat16
    )
    summed = (
        lax.psum_scatter(partial_value, "tp", scatter_dimension=1, tiled=True)
        .astype(jnp.float32)
        .astype(jnp.bfloat16)
    )
    summed = summed.reshape(experts_n, capacity, summed.shape[1])
    returned = lax.all_to_all(summed, "ep", split_axis=0, concat_axis=0, tiled=True)
    returned = returned.reshape(experts_n * capacity, returned.shape[2])
    picked = returned[dest_slot].astype(jnp.float32)
    route_weight = group_prob[:, None] * expert_prob / jnp.sum(expert_prob, axis=1, keepdims=True)
    expert_out = jnp.sum(
        picked.reshape(moe_rows, top_count, picked.shape[1]) * route_weight[:, :, None], axis=1
    )
    return (attend_out, expert_out.astype(jnp.bfloat16))


def solution(mesh):
    placed = (
        P("ep", None),
        P(),
        P(None, "tp"),
        P(None, "tp"),
        P(None, "tp"),
        P(),
        P(),
        P("tp"),
        P("tp", None),
        P("ep", None),
        P(),
        P("ep", None),
        P("ep"),
        P("ep", None),
        P("ep", None, "tp"),
        P("ep", None, "tp"),
        P("ep", "tp", None),
    )
    return jax.shard_map(
        per_device,
        mesh=mesh,
        in_specs=placed,
        out_specs=(P(("ep", "tp"), None), P("ep", "tp")),
        check_vma=False,
    )
```

profile of v0, /device:TPU:0, one launch (start us, length us, event | category | flops | bytes accessed | tf_op | source)
XLA Modules:
  0.0 207.4 jit_solution(12722982645366641306)
XLA Ops:
  7.2 3.6 %convert_element_type.89 = f32[384,2048]{1,0:T(8,128)} convert(bf16[384,2048]{1,0:T(8,128)(2,1)} %param.26) | non-fusion elementwise | flops 786432 | bytes 4718592 | tf_op jit(solution)/shard_map/convert_element_type | solution.py:27
  11.7 1.7 reduce-window.6
  14.3 3.4 %scatter_custom_fusion = s32[1152]{0:T(1024)S(1)} fusion(s32[768]{0:T(1024)S(1)} %fusion.40, s32[768]{0:T(1024)S(1)} %add_select_fusion, s32[]{:T(128)} %constant.107.clone.1), kind=kCustom, calls=%fused_computation.78 | custom fusion | bytes 4612 | tf_op jit(solution)/shard_map/scatter | solution.py:148
  17.7 0.8 dynamic-slice
  18.5 1.3 fusion.22
  19.8 4.2 %gather_fusion = bf16[1152,512]{1,0:T(8,128)(2,1)S(1)} fusion(bf16[385,512]{1,0:T(8,128)(2,1)S(1)} %concatenate.36, s32[2048]{0:T(1024)S(1)} %pad_clamp_fusion), kind=kCustom, calls=%fused_computation | custom fusion | bytes 2363904 | tf_op jit(solution)/shard_map/gather | solution.py:155
  24.1 36.2 %all_to_all.10 = bf16[8,144,512]{2,1,0:T(8,128)(2,1)} all-to-all(bf16[8,144,512]{2,1,0:T(8,128)(2,1)S(1)} %bitcast.69), channel_id=1, replica_groups=mesh['ep'=8,'tp'=4] {'ep'}, dimensions={0} | all-to-all | bytes 2359296 | tf_op jit(solution)/shard_map/all_to_all | solution.py:156
  60.4 36.2 %all-gather.2.cloned.1.call-done = bf16[8,144,2048]{2,1,0:T(8,128)(2,1)} async-done(((bf16[8,144,512]{2,1,0:T(8,128)(2,1)}), bf16[8,144,2048]{2,1,0:T(8,128)(2,1)}) %all-gather.2.cloned.1.call-update) | async-done | bytes 4718608 | tf_op jit(solution)/shard_map/all_gather | solution.py:157
  96.6 4.8 %fusion.19 = f32[1152,256]{1,0:T(8,128)} fusion(bf16[1152,2048]{1,0:T(8,128)(2,1)} %bitcast.79, bf16[1,2048,256]{2,1,0:T(8,128)(2,1)S(1)} %copy-done.9), kind=kOutput, calls=%fused_computation.33 | convolution fusion | flops 1207959552 | bytes 6946816 | tf_op jit(solution)/shard_map/dot_general | solution.py:159
  101.4 9.7 %convolution_convert_fusion = bf16[1152,2048]{1,0:T(8,128)(2,1)} fusion(bf16[1152,2048]{1,0:T(8,128)(2,1)} %bitcast.80, f32[1152,256]{1,0:T(8,128)} %fusion.19, bf16[1,256,2048]{2,1,0:T(8,128)(2,1)S(1)} %copy-done, bf16[1,2048,256]{2,1,0:T(8,128)(2,1)S(1)} %copy-done.10), kind=kOutput, calls=%fused_computation.3 | convolution fusion | flops 2420047872 | bytes 12713984 | tf_op jit(solution)/shard_map/dot_general | solution.py:162
  111.6 1.2 copy-done.2
  112.7 0.5 fusion.2
  113.2 2.0 multiply_reduce_fusion.3
  115.5 1.9 fusion.15
  117.4 0.7 pad_maximum_fusion.3
  118.1 3.9 %collective-permute-start = (bf16[2,128,128]{2,1,0:T(8,128)(2,1)}, bf16[2,128,128]{2,1,0:T(8,128)(2,1)}, u32[]{:S(2)}, u32[]{:S(2)}) collective-permute-start(bf16[2,128,128]{2,1,0:T(8,128)(2,1)} %get-tuple-element.8), channel_id=1, source_target_pairs={{0,4},{4,8},{8,12},{12,16},{16,20},{20,24},{24,28},{1,5},{5,9},{9,... | collective-permute-start | bytes 196616 | tf_op jit(solution)/shard_map/ppermute | solution.py:20
  122.0 1.5 collective-permute-start.1
  123.6 2.2 %multiply_reduce_fusion.2 = (f32[512,4]{0,1:T(4,128)S(1)}, f32[512,256]{0,1:T(8,128)S(1)}) fusion(bf16[2048,256]{1,0:T(8,128)(2,1)} %param.19, bf16[512,2048]{1,0:T(8,128)(2,1)S(1)} %copy-done.2, f32[2048]{0:T(1024)} %param.18, f32[512]{0:T(512)S(1)} %add_rsqrt_fusion.3), kind=kOutput, calls=%fused_computation.40 | convolution fusion | flops 541325312 | bytes 3688448 | tf_op jit(solution)/shard_map/dot_general | solution.py:86
  126.0 0.8 fusion.8
  126.9 1.6 collective-permute-done.1
  128.5 0.9 pad_maximum_fusion
  129.7 1.3 fusion.1
  131.1 1.4 fusion
  132.6 1.9 fusion.9
  134.5 2.1 %convolution_convert_fusion.1 = bf16[512,2048]{1,0:T(8,128)(2,1)} fusion(bf16[512,256]{0,1:T(8,128)(2,1)S(1)} %bitcast.71, bf16[256,2048]{1,0:T(8,128)(2,1)S(1)} %copy-done.3), kind=kOutput, calls=%fused_computation.16 | convolution fusion | flops 537919488 | bytes 3407872 | tf_op jit(solution)/shard_map/dot_general | solution.py:129
  136.7 22.5 %reduce-scatter.5.cloned.1.call-done = bf16[1152,512]{1,0:T(8,128)(2,1)} async-done(((bf16[1152,2048]{1,0:T(8,128)(2,1)}), bf16[1152,512]{1,0:T(8,128)(2,1)}) %reduce-scatter.5.cloned.1.call-update) | async-done | bytes 1179664 | tf_op jit(solution)/shard_map/reduce_scatter | solution.py:166
  159.2 5.5 %all-to-all-start.1 = ((bf16[8,144,512]{2,1,0:T(8,128)(2,1)}), bf16[8,144,512]{2,1,0:T(8,128)(2,1)S(1)}, u32[]{:S(2)}, u32[]{:S(2)}) async-start(bf16[8,144,512]{2,1,0:T(8,128)(2,1)} %bitcast.70), calls=%async_computation.3 | async-start | bytes 2359296 | tf_op jit(solution)/shard_map/all_to_all | solution.py:171
  164.7 0.8 copy.35
  165.5 27.5 %all-to-all-done.1 = bf16[8,144,512]{2,1,0:T(8,128)(2,1)S(1)} async-done(((bf16[8,144,512]{2,1,0:T(8,128)(2,1)}), bf16[8,144,512]{2,1,0:T(8,128)(2,1)S(1)}, u32[]{:S(2)}, u32[]{:S(2)}) %all-to-all-start.1) | async-done | bytes 1179680 | tf_op jit(solution)/shard_map/all_to_all | solution.py:171
  193.1 2.7 %gather_fusion.1 = bf16[768,512]{1,0:T(8,128)(2,1)S(1)} fusion(bf16[1152,512]{1,0:T(8,128)(2,1)S(1)} %bitcast.68, s32[1024]{0:T(1024)S(1)} %pad_clamp_fusion.1), kind=kCustom, calls=%fused_computation.1 | custom fusion | bytes 1575936 | tf_op jit(solution)/shard_map/gather | solution.py:173
  195.7 1.0 reshape.323
  196.7 4.1 %multiply_reduce_fusion.1 = bf16[384,512]{1,0:T(8,128)(2,1)} fusion(f32[384,2,512]{2,1,0:T(2,128)S(1)} %reshape.323, f32[384,2]{1,0:T(8,128)} %copy.35), kind=kLoop, calls=%fused_computation.19 | loop fusion | flops 589824 | bytes 1969152 | tf_op jit(solution)/shard_map/reduce_sum | solution.py:175
  (77 shorter events, 3.4 us)
Async XLA Ops:
  7.2 94.3 %copy-start = (bf16[1,256,2048]{2,1,0:T(8,128)(2,1)S(1)}, bf16[1,256,2048]{2,1,0:T(8,128)(2,1)}, u32[]{:S(2)}) copy-start(bf16[1,256,2048]{2,1,0:T(8,128)(2,1)} %param.33) | copy-start | bytes 3145732
  7.2 3.7 %copy-start.1 = (bf16[384,2048]{1,0:T(8,128)(2,1)S(1)}, bf16[384,2048]{1,0:T(8,128)(2,1)}, u32[]{:S(2)}) copy-start(bf16[384,2048]{1,0:T(8,128)(2,1)} %param.26) | copy-start | bytes 4718596
  7.2 89.4 %all-gather.2.cloned.1.call-start = ((), (), s32[]{:S(2)}) async-start(), calls=%async_computation.5 | async-start | bytes 5898240 | tf_op jit(solution)/shard_map/all_gather | solution.py:157
  7.2 4.0 %copy-start.5 = (s32[384,2]{0,1:T(2,128)S(1)}, s32[384,2]{0,1:T(2,128)}, u32[]{:S(2)}) copy-start(s32[384,2]{0,1:T(2,128)} %param.28) | copy-start | bytes 9220
  24.1 72.6 %copy-start.9 = (bf16[1,2048,256]{2,1,0:T(8,128)(2,1)S(1)}, bf16[1,2048,256]{2,1,0:T(8,128)(2,1)}, u32[]{:S(2)}) copy-start(bf16[1,2048,256]{2,1,0:T(8,128)(2,1)} %param.31) | copy-start | bytes 3145732
  60.3 98.8 %reduce-scatter.5.cloned.1.call-start = ((), (), s32[]{:S(2)}) async-start(), calls=%async_computation.6 | async-start | bytes 5898240 | tf_op jit(solution)/shard_map/reduce_scatter | solution.py:166
  96.6 4.8 %copy-start.10 = (bf16[1,2048,256]{2,1,0:T(8,128)(2,1)S(1)}, bf16[1,2048,256]{2,1,0:T(8,128)(2,1)}, u32[]{:S(2)}) copy-start(bf16[1,2048,256]{2,1,0:T(8,128)(2,1)} %param.32) | copy-start | bytes 3145732
  111.1 1.6 copy-start.2
  111.1 2.1 %copy-start.11 = (f32[2048]{0:T(1024)S(1)}, f32[2048]{0:T(1024)}, u32[]{:S(2)}) copy-start(f32[2048]{0:T(1024)} %param.18) | copy-start | bytes 24580
  111.2 89.7 %reduce-scatter.3.cloned.1.call-start = ((), (), s32[]{:S(2)}) async-start(), calls=%async_computation.4 | async-start | bytes 2621440 | tf_op jit(solution)/shard_map/reduce_scatter | solution.py:128
  112.7 2.5 %copy-start.7 = (f32[64]{0:T(128)S(1)}, f32[64]{0:T(128)}, u32[]{:S(2)}) copy-start(f32[64]{0:T(128)} %param.23) | copy-start | bytes 772
  117.4 8.4 %copy-start.8 = (f32[64]{0:T(128)S(1)}, f32[64]{0:T(128)}, u32[]{:S(2)}) copy-start(f32[64]{0:T(128)} %param.22) | copy-start | bytes 772
  118.1 8.8 %collective-permute-start = (bf16[2,128,128]{2,1,0:T(8,128)(2,1)}, bf16[2,128,128]{2,1,0:T(8,128)(2,1)}, u32[]{:S(2)}, u32[]{:S(2)}) collective-permute-start(bf16[2,128,128]{2,1,0:T(8,128)(2,1)} %get-tuple-element.8), channel_id=1, source_target_pairs={{0,4},{4,8},{8,12},{12,16},{16,20},{20,24},{24,28},{1,5},{5,9},{9,... | collective-permute-start | bytes 196616 | tf_op jit(solution)/shard_map/ppermute | solution.py:20
  122.0 6.5 %collective-permute-start.1 = (bf16[2,128,128]{2,1,0:T(8,128)(2,1)}, bf16[2,128,128]{2,1,0:T(8,128)(2,1)}, u32[]{:S(2)}, u32[]{:S(2)}) collective-permute-start(bf16[2,128,128]{2,1,0:T(8,128)(2,1)} %get-tuple-element.9), channel_id=1, source_target_pairs={{4,0},{8,4},{12,8},{16,12},{20,16},{24,20},{28,24},{5,1},{9,5},{13... | collective-permute-start | bytes 196616 | tf_op jit(solution)/shard_map/ppermute | solution.py:21
  123.5 3.2 %copy-start.12 = (f32[4]{0:T(128)S(1)}, f32[4]{0:T(128)}, u32[]{:S(2)}) copy-start(f32[4]{0:T(128)} %param.24) | copy-start | bytes 52
  132.6 2.0 copy-start.3
  136.6 28.0 %copy-start.4 = (f32[384,2]{0,1:T(2,128)S(1)}, f32[384,2]{0,1:T(2,128)}, u32[]{:S(2)}) copy-start(f32[384,2]{0,1:T(2,128)} %param.30) | copy-start | bytes 9220
  136.6 28.1 %copy-start.6 = (f32[384]{0:T(512)S(1)}, f32[384]{0:T(512)}, u32[]{:S(2)}) copy-start(f32[384]{0:T(512)} %param.29) | copy-start | bytes 4612
  159.2 33.9 %all-to-all-start.1 = ((bf16[8,144,512]{2,1,0:T(8,128)(2,1)}), bf16[8,144,512]{2,1,0:T(8,128)(2,1)S(1)}, u32[]{:S(2)}, u32[]{:S(2)}) async-start(bf16[8,144,512]{2,1,0:T(8,128)(2,1)} %bitcast.70), calls=%async_computation.3 | async-start | bytes 2359296 | tf_op jit(solution)/shard_map/all_to_all | solution.py:171
Sparse Core Ops, SparseCore 0:
  60.4 36.1 all-gather.1
  111.3 47.8 reduce-scatter.4
  162.3 31.1 reduce-scatter.2
where the time goes:
time: 208 us; the launch traced here: 207 us
  waiting for transfers between devices  88 us (42%)
  blocking collectives  36.2 us (17%)
  matrix products  25.9 us (12%)
  other arithmetic  16.5 us (8%)
  local copies, waits for them, and re-layouts  15.6 us (8%)
  between operations  14.2 us (7%)
  starting transfers between devices  11 us (5%)
    all_gather x1, waiting for transfers between devices, per_device(): col_piece = lax.all_gather(arrived, 'tp', axis=2, tiled=True)  36.2 us
    all_to_all x1, blocking collectives, per_device(): lax.all_to_all(outgoing, 'ep', split_axis=0, concat_axis=0, tiled=True)  36.2 us
    all_to_all x1, waiting for transfers between devices, per_device(): lax.all_to_all(summed, 'ep', split_axis=0, concat_axis=0, tiled=True)  27.5 us
    reduce_scatter x1, waiting for transfers between devices, per_device(): lax.psum_scatter(partial_value, 'tp', scatter_dimension=1, tiled=True)  22.5 us
    dot_general x1, matrix products, per_device(): jnp.dot(hidden, down_mat, preferred_element_type=jnp.float32)  9.69 us
    all_to_all x1, starting transfers between devices, per_device(): lax.all_to_all(summed, 'ep', split_axis=0, concat_axis=0, tiled=True)  5.52 us
    dot_general x1, matrix products, per_device(): gate_act = jnp.dot(rows_in, gate_mat, preferred_element_type=jnp.float32)  4.82 us
    gather x1, local copies, waits for them, and re-layouts, per_device(): outgoing = padded_rows[slot_tok].reshape(experts_n, capacity, col_width)  4.24 us
  transfers between devices with their start and end apart: 6, of which 4 were waited for; matrix products, arithmetic and copies ran while one was open for 12% of the time, Pallas kernels for 0%

commit v1 on v0

--- a/solution.py
+++ b/solution.py
@@ -153,7 +153,19 @@
     own_cols = lax.dynamic_slice_in_dim(moe_normed, lax.axis_index("tp") * col_width, col_width, 1)
     padded_rows = jnp.concatenate([own_cols, jnp.zeros((1, col_width), jnp.bfloat16)], axis=0)
     outgoing = padded_rows[slot_tok].reshape(experts_n, capacity, col_width)
-    arrived = lax.all_to_all(outgoing, "ep", split_axis=0, concat_axis=0, tiled=True)
+    ways, here = (lax.axis_size("ep"), lax.axis_index("ep"))
+    width_2 = outgoing.shape[0] // ways
+    shape = list(outgoing.shape)
+    shape[0] = width_2
+    height = shape[0]
+    shape[0] = height * ways
+    full = jnp.zeros(shape, outgoing.dtype)
+    for mask in range(ways):
+        part = lax.dynamic_slice_in_dim(outgoing, (here ^ mask) * width_2, width_2, axis=0)
+        if mask:
+            part = lax.ppermute(part, "ep", [(d, d ^ mask) for d in range(ways)])
+        full = lax.dynamic_update_slice_in_dim(full, part, (here ^ mask) * height, axis=0)
+    arrived = full
     col_piece = lax.all_gather(arrived, "tp", axis=2, tiled=True)
     rows_in = col_piece.reshape(experts_n * capacity, col_piece.shape[2])
     gate_act = jnp.dot(rows_in, gate_mat, preferred_element_type=jnp.float32)

time: 208 us -> 209 us (level)
  blocking collectives: 36.2 us -> 0 us
  waiting for transfers between devices: 88 us -> 106 us
  starting transfers between devices: 11 us -> 24.4 us
  local copies, waits for them, and re-layouts: 15.6 us -> 21.9 us
    all_to_all x1 -> x0, blocking collectives: 36.2 us -> none  [per_device(): lax.all_to_all(outgoing, 'ep', split_axis=0, concat_axis=0, tiled=True)]
    ppermute x0 -> x7, starting transfers between devices: none -> 13.3 us  [per_device(): part = lax.ppermute(part, 'ep', [(d, d ^ mask) for d in range(ways)])]
    ppermute x0 -> x7, waiting for transfers between devices: none -> 13 us  [per_device(): part = lax.ppermute(part, 'ep', [(d, d ^ mask) for d in range(ways)])]
    dynamic_update_slice x0 -> x7, local copies, waits for them, and re-layouts: none -> 4.65 us  [per_device(): lax.dynamic_update_slice_in_dim(full, part, (here ^ mask) * height, axis=0)]
    all_gather x1, waiting for transfers between devices: 36.2 us -> 40.3 us  [per_device(): col_piece = lax.all_gather(arrived, 'tp', axis=2, tiled=True)]
  transfers between devices with their start and end apart: 6 -> 13, of which waited for: 4 -> 6; matrix products, arithmetic and copies ran while one was open for 12% -> 14% of each run, Pallas kernels for 0% -> 0%
where the time goes in v1:
time: 209 us; the launch traced here: 208 us
  waiting for transfers between devices  106 us (51%)
  matrix products  24.8 us (12%)
  starting transfers between devices  24.4 us (12%)
  local copies, waits for them, and re-layouts  21.9 us (10%)
  other arithmetic  16.4 us (8%)
  between operations  14.3 us (7%)
    all_gather x1, waiting for transfers between devices, per_device(): col_piece = lax.all_gather(arrived, 'tp', axis=2, tiled=True)  40.3 us
    all_to_all x1, waiting for transfers between devices, per_device(): lax.all_to_all(summed, 'ep', split_axis=0, concat_axis=0, tiled=True)  27.6 us
    reduce_scatter x1, waiting for transfers between devices, per_device(): lax.psum_scatter(partial_value, 'tp', scatter_dimension=1, tiled=True)  23.5 us
    ppermute x7, starting transfers between devices, per_device(): part = lax.ppermute(part, 'ep', [(d, d ^ mask) for d in range(ways)])  13.3 us
    ppermute x7, waiting for transfers between devices, per_device(): part = lax.ppermute(part, 'ep', [(d, d ^ mask) for d in range(ways)])  13 us
    dot_general x1, matrix products, per_device(): jnp.dot(hidden, down_mat, preferred_element_type=jnp.float32)  9.68 us
    all_to_all x1, starting transfers between devices, per_device(): lax.all_to_all(summed, 'ep', split_axis=0, concat_axis=0, tiled=True)  5.5 us
    dot_general x1, matrix products, per_device(): gate_act = jnp.dot(rows_in, gate_mat, preferred_element_type=jnp.float32)  4.82 us
  transfers between devices with their start and end apart: 13, of which 6 were waited for; matrix products, arithmetic and copies ran while one was open for 14% of the time, Pallas kernels for 0%

profile of v1, /device:TPU:0, one launch (start us, length us, event | category | flops | bytes accessed | tf_op | source)
XLA Modules:
  0.0 208.1 jit_solution(14739808150016395222)
XLA Ops:
  7.3 3.6 %convert_element_type.89 = f32[384,2048]{1,0:T(8,128)} convert(bf16[384,2048]{1,0:T(8,128)(2,1)} %param.26) | non-fusion elementwise | flops 786432 | bytes 4718592 | tf_op jit(solution)/shard_map/convert_element_type | solution.py:27
  11.8 1.7 reduce-window.6
  14.3 3.4 %scatter_custom_fusion = s32[1152]{0:T(1024)S(1)} fusion(s32[768]{0:T(1024)S(1)} %fusion.38, s32[768]{0:T(1024)S(1)} %add_select_fusion, s32[]{:T(128)} %constant.115.clone.1), kind=kCustom, calls=%fused_computation.88 | custom fusion | bytes 4612 | tf_op jit(solution)/shard_map/scatter | solution.py:148
  18.6 1.3 fusion.20
  19.9 4.2 %gather_fusion = bf16[1152,512]{1,0:T(8,128)(2,1)S(1)} fusion(bf16[385,512]{1,0:T(8,128)(2,1)S(1)} %concatenate.36, s32[2048]{0:T(1024)S(1)} %pad_clamp_fusion), kind=kCustom, calls=%fused_computation | custom fusion | bytes 2363904 | tf_op jit(solution)/shard_map/gather | solution.py:155
  24.1 1.1 broadcast_in_dim.16
  26.0 3.0 %collective-permute-start.2 = (bf16[1,144,512]{2,1,0:T(8,128)(2,1)S(1)}, bf16[1,144,512]{2,1,0:T(8,128)(2,1)S(1)}, u32[]{:S(2)}, u32[]{:S(2)}) collective-permute-start(bf16[1,144,512]{2,1,0:T(8,128)(2,1)S(1)} %get-tuple-element.8), channel_id=1, source_target_pairs={{0,4},{4,0},{8,12},{12,8},{16,20},{20,16},{24,28},{28,24},{1,5},{5... | collective-permute-start | bytes 442376 | tf_op jit(solution)/shard_map/ppermute | solution.py:166
  28.9 1.6 collective-permute-start.3
  30.5 3.0 %collective-permute-start.5 = (bf16[1,144,512]{2,1,0:T(8,128)(2,1)S(1)}, bf16[1,144,512]{2,1,0:T(8,128)(2,1)S(1)}, u32[]{:S(2)}, u32[]{:S(2)}) collective-permute-start(bf16[1,144,512]{2,1,0:T(8,128)(2,1)S(1)} %get-tuple-element.5), channel_id=1, source_target_pairs={{0,16},{4,20},{8,24},{12,28},{16,0},{20,4},{24,8},{28,12},{1,17},{... | collective-permute-start | bytes 442376 | tf_op jit(solution)/shard_map/ppermute | solution.py:166
  33.5 1.3 collective-permute-start.6
  34.8 3.6 %collective-permute-start.7 = (bf16[1,144,512]{2,1,0:T(8,128)(2,1)S(1)}, bf16[1,144,512]{2,1,0:T(8,128)(2,1)S(1)}, u32[]{:S(2)}, u32[]{:S(2)}) collective-permute-start(bf16[1,144,512]{2,1,0:T(8,128)(2,1)S(1)} %get-tuple-element.3), channel_id=1, source_target_pairs={{0,24},{4,28},{8,16},{12,20},{16,8},{20,12},{24,0},{28,4},{1,25},{... | collective-permute-start | bytes 442376 | tf_op jit(solution)/shard_map/ppermute | solution.py:166
  39.1 1.8 collective-permute-done.3
  43.8 11.2 %collective-permute-done.6 = bf16[1,144,512]{2,1,0:T(8,128)(2,1)S(1)} collective-permute-done((bf16[1,144,512]{2,1,0:T(8,128)(2,1)S(1)}, bf16[1,144,512]{2,1,0:T(8,128)(2,1)S(1)}, u32[]{:S(2)}, u32[]{:S(2)}) %collective-permute-start.6) | collective-permute-done | bytes 147488 | tf_op jit(solution)/shard_map/ppermute | solution.py:166
  57.1 40.3 %all-gather.2.cloned.1.call-done = bf16[8,144,2048]{2,1,0:T(8,128)(2,1)} async-done(((bf16[8,144,512]{2,1,0:T(8,128)(2,1)}), bf16[8,144,2048]{2,1,0:T(8,128)(2,1)}) %all-gather.2.cloned.1.call-update) | async-done | bytes 4718608 | tf_op jit(solution)/shard_map/all_gather | solution.py:169
  97.4 4.8 %fusion.17 = f32[1152,256]{1,0:T(8,128)} fusion(bf16[1152,2048]{1,0:T(8,128)(2,1)} %bitcast.82, bf16[1,2048,256]{2,1,0:T(8,128)(2,1)S(1)} %copy-done.9), kind=kOutput, calls=%fused_computation.28 | convolution fusion | flops 1207959552 | bytes 6946816 | tf_op jit(solution)/shard_map/dot_general | solution.py:171
  102.2 9.7 %convolution_convert_fusion = bf16[1152,2048]{1,0:T(8,128)(2,1)} fusion(bf16[1,256,2048]{2,1,0:T(8,128)(2,1)S(1)} %copy-done, f32[1152,256]{1,0:T(8,128)} %fusion.17, bf16[1152,2048]{1,0:T(8,128)(2,1)} %bitcast.83, bf16[1,2048,256]{2,1,0:T(8,128)(2,1)S(1)} %copy-done.10), kind=kOutput, calls=%fused_computation.3 | convolution fusion | flops 2420047872 | bytes 12713984 | tf_op jit(solution)/shard_map/dot_general | solution.py:174
  112.5 1.0 copy-done.2
  115.3 1.8 fusion.9
  117.8 4.0 %collective-permute-start = (bf16[2,128,128]{2,1,0:T(8,128)(2,1)}, bf16[2,128,128]{2,1,0:T(8,128)(2,1)}, u32[]{:S(2)}, u32[]{:S(2)}) collective-permute-start(bf16[2,128,128]{2,1,0:T(8,128)(2,1)} %get-tuple-element.16), channel_id=1, source_target_pairs={{0,4},{4,8},{8,12},{12,16},{16,20},{20,24},{24,28},{1,5},{5,9},{9,... | collective-permute-start | bytes 196616 | tf_op jit(solution)/shard_map/ppermute | solution.py:20
  121.8 1.3 collective-permute-start.1
  123.1 2.2 %multiply_reduce_fusion.2 = (f32[512,4]{0,1:T(4,128)S(1)}, f32[512,256]{0,1:T(8,128)S(1)}) fusion(bf16[2048,256]{1,0:T(8,128)(2,1)} %param.19, bf16[512,2048]{1,0:T(8,128)(2,1)S(1)} %copy-done.2, f32[2048]{0:T(1024)S(1)} %copy-done.12, f32[512]{0:T(512)S(1)} %add_rsqrt_fusion.3), kind=kOutput, calls=%fused_computation.35 | convolution fusion | flops 541325312 | bytes 3688448 | tf_op jit(solution)/shard_map/dot_general | solution.py:86
  126.5 1.8 collective-permute-done.1
  129.5 1.3 fusion.1
  130.8 1.4 fusion
  132.3 1.9 fusion.8
  134.3 2.1 %convolution_convert_fusion.1 = bf16[512,2048]{1,0:T(8,128)(2,1)} fusion(bf16[512,256]{0,1:T(8,128)(2,1)S(1)} %bitcast.74, bf16[256,2048]{1,0:T(8,128)(2,1)S(1)} %copy-done.3), kind=kOutput, calls=%fused_computation.16 | convolution fusion | flops 537919488 | bytes 3407872 | tf_op jit(solution)/shard_map/dot_general | solution.py:129
  136.4 23.5 %reduce-scatter.5.cloned.1.call-done = bf16[1152,512]{1,0:T(8,128)(2,1)} async-done(((bf16[1152,2048]{1,0:T(8,128)(2,1)}), bf16[1152,512]{1,0:T(8,128)(2,1)}) %reduce-scatter.5.cloned.1.call-update) | async-done | bytes 1179664 | tf_op jit(solution)/shard_map/reduce_scatter | solution.py:178
  159.9 5.5 %all-to-all-start = ((bf16[8,144,512]{2,1,0:T(8,128)(2,1)}), bf16[8,144,512]{2,1,0:T(8,128)(2,1)S(1)}, u32[]{:S(2)}, u32[]{:S(2)}) async-start(bf16[8,144,512]{2,1,0:T(8,128)(2,1)} %bitcast.73), calls=%async_computation.2 | async-start | bytes 2359296 | tf_op jit(solution)/shard_map/all_to_all | solution.py:183
  166.3 27.6 %all-to-all-done = bf16[8,144,512]{2,1,0:T(8,128)(2,1)S(1)} async-done(((bf16[8,144,512]{2,1,0:T(8,128)(2,1)}), bf16[8,144,512]{2,1,0:T(8,128)(2,1)S(1)}, u32[]{:S(2)}, u32[]{:S(2)}) %all-to-all-start) | async-done | bytes 1179680 | tf_op jit(solution)/shard_map/all_to_all | solution.py:183
  193.8 2.7 %gather_fusion.1 = bf16[768,512]{1,0:T(8,128)(2,1)S(1)} fusion(bf16[1152,512]{1,0:T(8,128)(2,1)S(1)} %bitcast.71, s32[1024]{0:T(1024)S(1)} %pad_clamp_fusion.1), kind=kCustom, calls=%fused_computation.1 | custom fusion | bytes 1575936 | tf_op jit(solution)/shard_map/gather | solution.py:185
  196.5 1.0 reshape.323
  197.5 4.1 %multiply_reduce_fusion.1 = bf16[384,512]{1,0:T(8,128)(2,1)} fusion(f32[384,2,512]{2,1,0:T(2,128)S(1)} %reshape.323, f32[384,2]{1,0:T(8,128)} %copy.35), kind=kLoop, calls=%fused_computation.17 | loop fusion | flops 589824 | bytes 1969152 | tf_op jit(solution)/shard_map/reduce_sum | solution.py:187
  (101 shorter events, 15.2 us)
Async XLA Ops:
  7.2 95.1 %copy-start = (bf16[1,256,2048]{2,1,0:T(8,128)(2,1)S(1)}, bf16[1,256,2048]{2,1,0:T(8,128)(2,1)}, u32[]{:S(2)}) copy-start(bf16[1,256,2048]{2,1,0:T(8,128)(2,1)} %param.33) | copy-start | bytes 3145732
  7.2 90.2 %all-gather.2.cloned.1.call-start = ((), (), s32[]{:S(2)}) async-start(), calls=%async_computation.4 | async-start | bytes 5898240 | tf_op jit(solution)/shard_map/all_gather | solution.py:169
  7.3 3.6 %copy-start.1 = (bf16[384,2048]{1,0:T(8,128)(2,1)S(1)}, bf16[384,2048]{1,0:T(8,128)(2,1)}, u32[]{:S(2)}) copy-start(bf16[384,2048]{1,0:T(8,128)(2,1)} %param.26) | copy-start | bytes 4718596
  7.3 4.0 %copy-start.5 = (s32[384,2]{0,1:T(2,128)S(1)}, s32[384,2]{0,1:T(2,128)}, u32[]{:S(2)}) copy-start(s32[384,2]{0,1:T(2,128)} %param.28) | copy-start | bytes 9220
  26.0 71.4 %copy-start.9 = (bf16[1,2048,256]{2,1,0:T(8,128)(2,1)S(1)}, bf16[1,2048,256]{2,1,0:T(8,128)(2,1)}, u32[]{:S(2)}) copy-start(bf16[1,2048,256]{2,1,0:T(8,128)(2,1)} %param.31) | copy-start | bytes 3145732
  26.0 8.8 %collective-permute-start.2 = (bf16[1,144,512]{2,1,0:T(8,128)(2,1)S(1)}, bf16[1,144,512]{2,1,0:T(8,128)(2,1)S(1)}, u32[]{:S(2)}, u32[]{:S(2)}) collective-permute-start(bf16[1,144,512]{2,1,0:T(8,128)(2,1)S(1)} %get-tuple-element.8), channel_id=1, source_target_pairs={{0,4},{4,0},{8,12},{12,8},{16,20},{20,16},{24,28},{28,24},{1,5},{5... | collective-permute-start | bytes 442376 | tf_op jit(solution)/shard_map/ppermute | solution.py:166
  28.9 11.9 %collective-permute-start.3 = (bf16[1,144,512]{2,1,0:T(8,128)(2,1)S(1)}, bf16[1,144,512]{2,1,0:T(8,128)(2,1)S(1)}, u32[]{:S(2)}, u32[]{:S(2)}) collective-permute-start(bf16[1,144,512]{2,1,0:T(8,128)(2,1)S(1)} %get-tuple-element.7), channel_id=1, source_target_pairs={{0,8},{4,12},{8,0},{12,4},{16,24},{20,28},{24,16},{28,20},{1,9},{5... | collective-permute-start | bytes 442376 | tf_op jit(solution)/shard_map/ppermute | solution.py:166
  30.5 11.9 %collective-permute-start.4 = (bf16[1,144,512]{2,1,0:T(8,128)(2,1)S(1)}, bf16[1,144,512]{2,1,0:T(8,128)(2,1)S(1)}, u32[]{:S(2)}, u32[]{:S(2)}) collective-permute-start(bf16[1,144,512]{2,1,0:T(8,128)(2,1)S(1)} %get-tuple-element.6), channel_id=1, source_target_pairs={{0,12},{4,8},{8,4},{12,0},{16,28},{20,24},{24,20},{28,16},{1,13},{... | collective-permute-start | bytes 442376 | tf_op jit(solution)/shard_map/ppermute | solution.py:166
  30.5 12.6 %collective-permute-start.5 = (bf16[1,144,512]{2,1,0:T(8,128)(2,1)S(1)}, bf16[1,144,512]{2,1,0:T(8,128)(2,1)S(1)}, u32[]{:S(2)}, u32[]{:S(2)}) collective-permute-start(bf16[1,144,512]{2,1,0:T(8,128)(2,1)S(1)} %get-tuple-element.5), channel_id=1, source_target_pairs={{0,16},{4,20},{8,24},{12,28},{16,0},{20,4},{24,8},{28,12},{1,17},{... | collective-permute-start | bytes 442376 | tf_op jit(solution)/shard_map/ppermute | solution.py:166
  33.5 21.5 %collective-permute-start.6 = (bf16[1,144,512]{2,1,0:T(8,128)(2,1)S(1)}, bf16[1,144,512]{2,1,0:T(8,128)(2,1)S(1)}, u32[]{:S(2)}, u32[]{:S(2)}) collective-permute-start(bf16[1,144,512]{2,1,0:T(8,128)(2,1)S(1)} %get-tuple-element.4), channel_id=1, source_target_pairs={{0,20},{4,16},{8,28},{12,24},{16,4},{20,0},{24,12},{28,8},{1,21},{... | collective-permute-start | bytes 442376 | tf_op jit(solution)/shard_map/ppermute | solution.py:166
  34.8 20.9 %collective-permute-start.7 = (bf16[1,144,512]{2,1,0:T(8,128)(2,1)S(1)}, bf16[1,144,512]{2,1,0:T(8,128)(2,1)S(1)}, u32[]{:S(2)}, u32[]{:S(2)}) collective-permute-start(bf16[1,144,512]{2,1,0:T(8,128)(2,1)S(1)} %get-tuple-element.3), channel_id=1, source_target_pairs={{0,24},{4,28},{8,16},{12,20},{16,8},{20,12},{24,0},{28,4},{1,25},{... | collective-permute-start | bytes 442376 | tf_op jit(solution)/shard_map/ppermute | solution.py:166
  40.9 15.5 %collective-permute-start.8 = (bf16[1,144,512]{2,1,0:T(8,128)(2,1)S(1)}, bf16[1,144,512]{2,1,0:T(8,128)(2,1)S(1)}, u32[]{:S(2)}, u32[]{:S(2)}) collective-permute-start(bf16[1,144,512]{2,1,0:T(8,128)(2,1)S(1)} %get-tuple-element.2), channel_id=1, source_target_pairs={{0,28},{4,24},{8,20},{12,16},{16,12},{20,8},{24,4},{28,0},{1,29},{... | collective-permute-start | bytes 442376 | tf_op jit(solution)/shard_map/ppermute | solution.py:166
  57.0 102.9 %reduce-scatter.5.cloned.1.call-start = ((), (), s32[]{:S(2)}) async-start(), calls=%async_computation.5 | async-start | bytes 5898240 | tf_op jit(solution)/shard_map/reduce_scatter | solution.py:178
  97.4 4.8 %copy-start.10 = (bf16[1,2048,256]{2,1,0:T(8,128)(2,1)S(1)}, bf16[1,2048,256]{2,1,0:T(8,128)(2,1)}, u32[]{:S(2)}) copy-start(bf16[1,2048,256]{2,1,0:T(8,128)(2,1)} %param.32) | copy-start | bytes 3145732
  111.9 1.6 copy-start.2
  111.9 2.1 copy-start.12
  111.9 89.6 %reduce-scatter.3.cloned.1.call-start = ((), (), s32[]{:S(2)}) async-start(), calls=%async_computation.3 | async-start | bytes 2621440 | tf_op jit(solution)/shard_map/reduce_scatter | solution.py:128
  112.2 1.8 copy-start.11
  114.0 1.0 copy-start.7
  117.8 8.7 %collective-permute-start = (bf16[2,128,128]{2,1,0:T(8,128)(2,1)}, bf16[2,128,128]{2,1,0:T(8,128)(2,1)}, u32[]{:S(2)}, u32[]{:S(2)}) collective-permute-start(bf16[2,128,128]{2,1,0:T(8,128)(2,1)} %get-tuple-element.16), channel_id=1, source_target_pairs={{0,4},{4,8},{8,12},{12,16},{16,20},{20,24},{24,28},{1,5},{5,9},{9,... | collective-permute-start | bytes 196616 | tf_op jit(solution)/shard_map/ppermute | solution.py:20
  121.8 6.5 %collective-permute-start.1 = (bf16[2,128,128]{2,1,0:T(8,128)(2,1)}, bf16[2,128,128]{2,1,0:T(8,128)(2,1)}, u32[]{:S(2)}, u32[]{:S(2)}) collective-permute-start(bf16[2,128,128]{2,1,0:T(8,128)(2,1)} %get-tuple-element.17), channel_id=1, source_target_pairs={{4,0},{8,4},{12,8},{16,12},{20,16},{24,20},{28,24},{5,1},{9,5},{13... | collective-permute-start | bytes 196616 | tf_op jit(solution)/shard_map/ppermute | solution.py:21
  123.1 2.3 %copy-start.8 = (f32[64]{0:T(128)S(1)}, f32[64]{0:T(128)}, u32[]{:S(2)}) copy-start(f32[64]{0:T(128)} %param.22) | copy-start | bytes 772
  125.4 1.0 copy-start.13
  132.3 2.0 copy-start.3
  136.4 29.0 %copy-start.4 = (f32[384,2]{0,1:T(2,128)S(1)}, f32[384,2]{0,1:T(2,128)}, u32[]{:S(2)}) copy-start(f32[384,2]{0,1:T(2,128)} %param.30) | copy-start | bytes 9220
  136.4 29.1 %copy-start.6 = (f32[384]{0:T(512)S(1)}, f32[384]{0:T(512)}, u32[]{:S(2)}) copy-start(f32[384]{0:T(512)} %param.29) | copy-start | bytes 4612
  159.9 33.9 %all-to-all-start = ((bf16[8,144,512]{2,1,0:T(8,128)(2,1)}), bf16[8,144,512]{2,1,0:T(8,128)(2,1)S(1)}, u32[]{:S(2)}, u32[]{:S(2)}) async-start(bf16[8,144,512]{2,1,0:T(8,128)(2,1)} %bitcast.73), calls=%async_computation.2 | async-start | bytes 2359296 | tf_op jit(solution)/shard_map/all_to_all | solution.py:183
Sparse Core Ops, SparseCore 0:
  57.1 40.1 all-gather.1
  112.0 47.7 reduce-scatter.4
  163.0 31.1 reduce-scatter.2
